TPU v7x, 32 devices: a whole 2x2x4 slice. The times are simulated.
32 devices in a mesh: ep: 8 (over z, core), tp: 4 (over y, x).
Axes of the slice: x: 2, y: 2, z: 4, core: 2. Of those that a mesh axis runs over, the one named last changes fastest.
Arguments:
- tokens: bfloat16 [1024, 4096], P('ep', 'tp'), may hold values from -6 to 6
- out_grad: bfloat16 [1024, 4096], P('ep', 'tp'), may hold values from -1.5 to 1.5
- routes: int32 [1024, 2], P('ep'), may hold values from 0 to 7, all different within a row; in each aligned block of 128 rows (0 to 127, 128 to 255, ...) at most 40 rows name the same one
- route_weights: float32 [1024, 2], P('ep'), may hold values from 0.2 to 1.2
- gate_proj: bfloat16 [8, 1024, 4096], P('ep', 'tp'), may hold values from -0.09375 to 0.09375
- up_proj: bfloat16 [8, 1024, 4096], P('ep', 'tp'), may hold values from -0.09375 to 0.09375
- down_proj: bfloat16 [8, 1024, 4096], P('ep', 'tp'), may hold values from -0.1875 to 0.1875
- shared_hidden: bfloat16 [1024, 1024], P('ep'), may hold values from -6 to 6
Outputs:
- token_grad: bfloat16 [1024, 4096], P('ep', 'tp')
- weight_grad: float32 [1024, 2], P('ep')
- gate_grad: bfloat16 [8, 1024, 4096], P('ep', 'tp')
- up_grad: bfloat16 [8, 1024, 4096], P('ep', 'tp')
- down_grad: bfloat16 [8, 1024, 4096], P('ep', 'tp')
- shared_grad: float32 [1024, 4096], P('ep', 'tp')
Inputs may be any that keep to these rules, and one draw needn't show every extreme that they name: Within each block of 128 consecutive tokens, no expert is named by more than 40 routes, and in some blocks one expert is named by exactly 40. The 2 experts of one token differ.
All inputs are finite; a program needn't handle non-finite values.
Results may differ from a plain program's by a relative error of at most 0.0065.
Values may be sent and summed in bfloat16 or wider, within the bound.
A program may use at most 64 MiB of HBM per device.

v0:
```python
import jax
import jax.numpy as jnp
from jax import lax
from jax.sharding import PartitionSpec as P


def slot_tables(routes, num_experts, capacity):
    tok_rows, per_token = routes.shape
    route_count = tok_rows * per_token
    flat_routes = routes.reshape(-1)
    expert_ids = lax.broadcasted_iota(jnp.int32, (route_count, num_experts), 1)
    onehot = (flat_routes[:, None] == expert_ids).astype(jnp.int32)
    slot_rank = jnp.sum((jnp.cumsum(onehot, axis=0) - 1) * onehot, axis=1)
    slot_of_route = flat_routes * capacity + slot_rank
    slot_ids = lax.broadcasted_iota(jnp.int32, (num_experts * capacity, route_count), 0)
    route_ids = lax.broadcasted_iota(jnp.int32, (num_experts * capacity, route_count), 1)
    matches = slot_ids == slot_of_route[None, :]
    route_of_slot = jnp.sum(jnp.where(matches, route_ids, 0), axis=1)
    filled = jnp.any(matches, axis=1)
    return (slot_of_route, route_of_slot, filled)


def local(tokens, out_grad, routes, route_weights, gate_proj, up_proj, down_proj, shared_hidden):
    ep_count = lax.axis_size("ep")
    tp_count = lax.axis_size("tp")
    local_experts = gate_proj.shape[0]
    num_experts = local_experts * ep_count
    tok_rows, per_token = routes.shape
    capacity = max(2, 5 * tok_rows * per_token // (4 * num_experts))
    slot_of_route, route_of_slot, filled = slot_tables(routes, num_experts, capacity)
    token_of_slot = route_of_slot // per_token
    zero_value = jnp.zeros((), jnp.bfloat16)
    slot_weight = jnp.where(filled, route_weights.reshape(-1)[route_of_slot], 0.0)
    slot_weight = slot_weight.astype(jnp.bfloat16).reshape(ep_count, local_experts, capacity)
    layout = (ep_count, local_experts, capacity, -1)
    sent_tokens = jnp.where(filled[:, None], tokens[token_of_slot], zero_value).reshape(layout)
    sent_grads = jnp.where(filled[:, None], out_grad[token_of_slot], zero_value).reshape(layout)
    part_tokens, part_grads, weights_in = (
        lax.all_to_all(sent_tokens, "ep", split_axis=0, concat_axis=2, tiled=True),
        lax.all_to_all(sent_grads, "ep", split_axis=0, concat_axis=2, tiled=True),
        lax.all_to_all(slot_weight, "ep", split_axis=0, concat_axis=2, tiled=True),
    )
    rows_in, grads_in = (
        lax.all_gather(part_tokens, "tp", axis=3, tiled=True),
        lax.all_gather(part_grads, "tp", axis=3, tiled=True),
    )
    rows_in = rows_in[0]
    grads_in = grads_in[0]
    slot_scale = weights_in[0].astype(jnp.float32)
    pre_gate = jnp.einsum("lrd,lfd->lrf", rows_in, gate_proj, preferred_element_type=jnp.float32)
    pre_up = jnp.einsum("lrd,lfd->lrf", rows_in, up_proj, preferred_element_type=jnp.float32)
    squash = jax.nn.sigmoid(pre_gate)
    activated = pre_gate * squash
    hidden = (activated * pre_up).astype(jnp.bfloat16)
    back_grad = jnp.einsum("lrd,lfd->lrf", grads_in, down_proj, preferred_element_type=jnp.float32)
    partial_products = jnp.sum(hidden.astype(jnp.float32) * back_grad, axis=2)
    hidden_grad = slot_scale[:, :, None] * back_grad
    scaled_hidden = (slot_scale[:, :, None] * hidden.astype(jnp.float32)).astype(jnp.bfloat16)
    gate_delta = (hidden_grad * pre_up * squash * (1.0 + pre_gate * (1.0 - squash))).astype(
        jnp.bfloat16
    )
    up_delta = (hidden_grad * activated).astype(jnp.bfloat16)
    gate_grad = jnp.einsum(
        "lrf,lrd->lfd", gate_delta, rows_in, preferred_element_type=jnp.float32
    ).astype(jnp.bfloat16)
    up_grad = jnp.einsum(
        "lrf,lrd->lfd", up_delta, rows_in, preferred_element_type=jnp.float32
    ).astype(jnp.bfloat16)
    down_grad = jnp.einsum(
        "lrf,lrd->lfd", scaled_hidden, grads_in, preferred_element_type=jnp.float32
    ).astype(jnp.bfloat16)
    partial_rows = jnp.einsum(
        "lrf,lfd->lrd", gate_delta, gate_proj, preferred_element_type=jnp.float32
    )
    partial_rows = partial_rows + jnp.einsum(
        "lrf,lfd->lrd", up_delta, up_proj, preferred_element_type=jnp.float32
    )
    partial_rows = partial_rows.astype(jnp.bfloat16)
    gathered = lax.all_to_all(partial_rows, "tp", split_axis=2, concat_axis=0, tiled=True)
    gathered = gathered.reshape((tp_count,) + partial_rows.shape[:2] + (-1,))
    summed = jnp.sum(gathered, axis=0, dtype=jnp.float32)
    products = lax.psum(partial_products, "tp")
    slot_rows, slot_products = (
        lax.all_to_all(summed[None], "ep", split_axis=2, concat_axis=0, tiled=True),
        lax.all_to_all(products[None], "ep", split_axis=2, concat_axis=0, tiled=True),
    )
    feature_width = slot_rows.shape[-1]
    slot_rows = slot_rows.reshape(num_experts * capacity, feature_width)
    route_rows = slot_rows[slot_of_route].reshape(tok_rows, per_token, feature_width)
    token_grad = jnp.sum(route_rows, axis=1).astype(jnp.bfloat16)
    weight_grad = slot_products.reshape(-1)[slot_of_route].reshape(tok_rows, per_token)
    shared_grad = lax.psum_scatter(
        lax.dot_general(
            shared_hidden, out_grad, (((0,), (0,)), ((), ())), preferred_element_type=jnp.float32
        ),
        "ep",
        scatter_dimension=0,
        tiled=True,
    )
    return (token_grad, weight_grad, gate_grad, up_grad, down_grad, shared_grad)


def solution(mesh):
    return jax.shard_map(
        local,
        mesh=mesh,
        in_specs=(
            P("ep", "tp"),
            P("ep", "tp"),
            P("ep", None),
            P("ep", None),
            P("ep", "tp", None),
            P("ep", "tp", None),
            P("ep", "tp", None),
            P("ep", None),
        ),
        out_specs=(
            P("ep", "tp"),
            P("ep", None),
            P("ep", "tp", None),
            P("ep", "tp", None),
            P("ep", "tp", None),
            P("ep", "tp"),
        ),
        check_vma=False,
    )
```

profile of v0, /device:TPU:0, one launch (start us, length us, event | category | flops | bytes accessed | tf_op | source)
XLA Modules:
  0.0 350.5 jit_solution(12991959504227618092)
XLA Ops:
  8.1 1.0 copy.50
  9.3 0.6 reduce-window.6
  9.9 0.2 slice_reduce_fusion
  10.3 0.2 select_reduce_fusion
  10.4 0.2 fusion.23
  10.6 2.6 gather_fusion.1
  13.3 2.6 gather_fusion.2
  16.0 1.4 broadcast_select_fusion.1
  17.5 24.5 %all_to_all.60 = bf16[8,1,40,1024]{3,2,1,0:T(8,128)(2,1)} all-to-all(bf16[8,1,40,1024]{3,2,1,0:T(8,128)(2,1)S(1)} %get-tuple-element.43), channel_id=1, replica_groups=mesh['ep'=8,'tp'=4] {'ep'}, dimensions={0} | all-to-all | bytes 1310720 | tf_op jit(solution)/shard_map/all_to_all | solution.py:39
  42.1 21.2 %all_to_all.61 = bf16[8,1,40,1024]{3,2,1,0:T(8,128)(2,1)} all-to-all(bf16[8,1,40,1024]{3,2,1,0:T(8,128)(2,1)S(1)} %get-tuple-element.42), channel_id=1, replica_groups=mesh['ep'=8,'tp'=4] {'ep'}, dimensions={0} | all-to-all | bytes 1310720 | tf_op jit(solution)/shard_map/all_to_all | solution.py:40
  63.4 2.8 fusion.30
  66.2 0.7 copy-done.10
  67.1 2.4 gather_fusion
  69.6 8.1 %all_to_all.62 = bf16[8,1,40]{2,1,0:T(2,128)(2,1)S(1)} all-to-all(bf16[8,1,40]{2,1,0:T(2,128)(2,1)S(1)} %convert_element_type.110), channel_id=1, replica_groups=mesh['ep'=8,'tp'=4] {'ep'}, dimensions={0} | all-to-all | bytes 1280 | tf_op jit(solution)/shard_map/all_to_all | solution.py:41
  77.8 2.8 all-gather.5.cloned.1.call-done
  80.6 2.8 fusion.7
  83.4 0.4 copy-done.6
  83.9 0.9 fusion.9
  84.8 37.3 %all-gather.3.cloned.1.call-done = bf16[1,1,320,4096]{3,2,1,0:T(8,128)(2,1)} async-done(((bf16[1,1,320,1024]{3,2,1,0:T(8,128)(2,1)}), bf16[1,1,320,4096]{3,2,1,0:T(8,128)(2,1)}) %all-gather.3.cloned.1.call-update) | async-done | bytes 2621456 | tf_op jit(solution)/shard_map/all_gather | solution.py:45
  122.0 3.4 fusion.20
  125.4 0.8 fusion.14
  126.3 0.7 copy-done.7
  127.0 2.4 fusion.1
  129.4 14.3 %copy.56 = bf16[1,320,4096]{1,0,2:T(2,128)(2,1)} copy(bf16[1,320,4096]{2,1,0:T(8,128)(2,1)} %fusion.1) | data formatting | bytes 5242880 | tf_op jit(solution)/shard_map/convert_element_type | solution.py:78
  143.7 0.5 broadcast.230
  144.3 68.8 %reduce.16 = bf16[4096,320]{1,0:T(8,128)(2,1)} reduce(bf16[4096,1,320]{2,1,0:T(2,128)(2,1)} %bitcast.67, bf16[]{:T(256)} %broadcast.230), dimensions={1}, to_apply=%bitcast.53.reduce_sub_computation | reduce | bytes 5242882
  213.0 6.1 %reshape.388 = bf16[4,2,163840]{2,1,0:T(2,128)(2,1)} reshape(bf16[4096,320]{1,0:T(8,128)(2,1)} %reduce.16) | data formatting | bytes 5242880
  219.2 4.6 %all-to-all-start.3 = ((bf16[4,2,163840]{2,1,0:T(2,128)(2,1)}), bf16[4,2,163840]{2,1,0:T(2,128)(2,1)}, u32[]{:S(2)}, u32[]{:S(2)}) async-start(bf16[4,2,163840]{2,1,0:T(2,128)(2,1)} %reshape.388), calls=%async_computation.3 | async-start | bytes 5242880 | tf_op jit(solution)/shard_map/all_to_all | solution.py:79
  223.8 33.7 %psum.7 = f32[1,1,320]{2,1,0:T(1,128)S(1)} all-reduce(f32[1,1,320]{2,1,0:T(1,128)S(1)} %broadcast_in_dim.48), channel_id=1, replica_groups=mesh['ep'=8,'tp'=4] {'tp'}, use_global_device_ids=true, to_apply=%region_8.9 | all-reduce | flops 320 | bytes 2560 | tf_op jit(solution)/shard_map/psum | solution.py:82
  257.5 0.8 copy.59
  258.3 4.6 %all-to-all-start.5 = ((f32[1,1,320]{1,0,2:T(1,128)}), f32[1,1,320]{1,0,2:T(1,128)S(1)}, u32[]{:S(2)}, u32[]{:S(2)}) async-start(f32[1,1,320]{1,0,2:T(1,128)} %copy.59), calls=%async_computation.5 | async-start | bytes 327680 | tf_op jit(solution)/shard_map/all_to_all | solution.py:85
  262.9 7.6 %reshape.389 = bf16[4096,1,320]{2,1,0:T(2,128)(2,1)} reshape(bf16[4,2,163840]{2,1,0:T(2,128)(2,1)} %all-to-all-done.3) | data formatting | bytes 5242880
  270.5 14.0 %copy.57 = bf16[1,320,4096]{2,1,0:T(8,128)(2,1)} copy(bf16[1,320,4096]{1,0,2:T(2,128)(2,1)} %bitcast.68) | data formatting | bytes 5242880 | tf_op jit(solution)/shard_map/all_to_all | solution.py:79
  284.5 7.3 %reshape.336 = f32[320,4,1024]{2,1,0:T(4,128)} reshape(bf16[1,320,4096]{2,1,0:T(8,128)(2,1)} %copy.57) | data formatting | bytes 7864320 | tf_op jit(solution)/shard_map/convert_element_type | solution.py:81
  291.8 5.7 %reduce_sum.54 = f32[320,1024]{1,0:T(8,128)S(1)} reduce(f32[320,4,1024]{2,1,0:T(4,128)} %reshape.336, f32[]{:T(128)} %constant.33.clone.1), dimensions={1}, to_apply=%region_5.6 | reduce | flops 983040 | bytes 6553604 | tf_op jit(solution)/shard_map/reduce_sum | solution.py:81
  297.5 2.0 broadcast_in_dim.47
  299.5 5.1 %all-to-all-start.4 = ((f32[1,1,320,1024]{3,1,0,2:T(1,128)}), f32[1,1,320,1024]{3,1,0,2:T(1,128)S(1)}, u32[]{:S(2)}, u32[]{:S(2)}) async-start(f32[1,1,320,1024]{3,1,0,2:T(1,128)} %broadcast_in_dim.47), calls=%async_computation.4 | async-start | bytes 2621440 | tf_op jit(solution)/shard_map/all_to_all | solution.py:84
  304.9 4.3 %fusion.2 = bf16[1,256,4096]{2,1,0:T(8,128)(2,1)} fusion(bf16[320,256]{1,0:T(8,128)(2,1)S(1)} %get-tuple-element.40, bf16[1,1,320,4096]{3,2,1,0:T(8,128)(2,1)} %all-gather.5.cloned.1.call-done), kind=kOutput, calls=%fused_computation.11 | convolution fusion | flops 672137216 | bytes 4882432 | tf_op jit(solution)/shard_map/lrf,lrd->lfd/dot_general | solution.py:63
  309.3 4.5 %fusion.3 = bf16[1,256,4096]{2,1,0:T(8,128)(2,1)} fusion(bf16[320,256]{1,0:T(8,128)(2,1)S(1)} %get-tuple-element.41, bf16[1,1,320,4096]{3,2,1,0:T(8,128)(2,1)} %all-gather.5.cloned.1.call-done), kind=kOutput, calls=%fused_computation.12 | convolution fusion | flops 672137216 | bytes 4882432 | tf_op jit(solution)/shard_map/lrf,lrd->lfd/dot_general | solution.py:66
  313.7 2.7 fusion.4
  316.4 1.1 reduce.9
  317.5 1.9 gather_fusion.4
  319.6 0.6 copy.60
  320.2 16.6 %all-to-all-done.4 = f32[1,1,320,1024]{3,1,0,2:T(1,128)S(1)} async-done(((f32[1,1,320,1024]{3,1,0,2:T(1,128)}), f32[1,1,320,1024]{3,1,0,2:T(1,128)S(1)}, u32[]{:S(2)}, u32[]{:S(2)}) %all-to-all-start.4) | async-done | bytes 1310752 | tf_op jit(solution)/shard_map/all_to_all | solution.py:84
  336.8 0.3 copy.63
  337.1 2.0 gather_fusion.3
  339.1 1.8 reshape.331
  341.0 2.1 reduce_sum.56
  (51 shorter events, 1.6 us)
Async XLA Ops:
  8.0 72.6 %copy-start = (bf16[1,256,4096]{2,1,0:T(8,128)(2,1)S(1)}, bf16[1,256,4096]{2,1,0:T(8,128)(2,1)}, u32[]{:S(2)}) copy-start(bf16[1,256,4096]{2,1,0:T(8,128)(2,1)} %param.12) | copy-start | bytes 6291460
  8.0 2.6 copy-start.2
  8.0 72.6 %all-gather.5.cloned.1.call-start = ((), (), s32[]{:S(2)}) async-start(), calls=%async_computation.8 | async-start | bytes 3276800 | tf_op jit(solution)/shard_map/all_gather | solution.py:44
  10.6 2.7 copy-start.3
  17.5 45.9 %copy-start.8 = (bf16[128,1024]{1,0:T(8,128)(2,1)S(1)}, bf16[128,1024]{1,0:T(8,128)(2,1)}, u32[]{:S(2)}) copy-start(bf16[128,1024]{1,0:T(8,128)(2,1)} %param.15) | copy-start | bytes 786436
  42.0 80.0 %all-gather.3.cloned.1.call-start = ((), (), s32[]{:S(2)}) async-start(), calls=%async_computation.7 | async-start | bytes 3276800 | tf_op jit(solution)/shard_map/all_gather | solution.py:45
  63.3 279.7 %reduce-scatter.2.cloned.1.call-start = ((), (), s32[]{:S(2)}) async-start(), calls=%async_computation.9 | async-start | bytes 4718592 | tf_op jit(solution)/shard_map/reduce_scatter | solution.py:92
  66.2 0.7 copy-start.10
  80.6 2.8 copy-start.4
  80.6 3.2 copy-start.6
  125.4 1.6 copy-start.7
  219.2 39.1 %all-to-all-start.3 = ((bf16[4,2,163840]{2,1,0:T(2,128)(2,1)}), bf16[4,2,163840]{2,1,0:T(2,128)(2,1)}, u32[]{:S(2)}, u32[]{:S(2)}) async-start(bf16[4,2,163840]{2,1,0:T(2,128)(2,1)} %reshape.388), calls=%async_computation.3 | async-start | bytes 5242880 | tf_op jit(solution)/shard_map/all_to_all | solution.py:79
  258.3 41.2 %all-to-all-start.5 = ((f32[1,1,320]{1,0,2:T(1,128)}), f32[1,1,320]{1,0,2:T(1,128)S(1)}, u32[]{:S(2)}, u32[]{:S(2)}) async-start(f32[1,1,320]{1,0,2:T(1,128)} %copy.59), calls=%async_computation.5 | async-start | bytes 327680 | tf_op jit(solution)/shard_map/all_to_all | solution.py:85
  297.5 7.1 %copy-start.9 = (s32[128,2]{0,1:T(2,128)S(1)}, s32[128,2]{0,1:T(2,128)}, u32[]{:S(2)}) copy-start(s32[128,2]{0,1:T(2,128)} %param.10) | copy-start | bytes 3076
  299.5 37.3 %all-to-all-start.4 = ((f32[1,1,320,1024]{3,1,0,2:T(1,128)}), f32[1,1,320,1024]{3,1,0,2:T(1,128)S(1)}, u32[]{:S(2)}, u32[]{:S(2)}) async-start(f32[1,1,320,1024]{3,1,0,2:T(1,128)} %broadcast_in_dim.47), calls=%async_computation.4 | async-start | bytes 2621440 | tf_op jit(solution)/shard_map/all_to_all | solution.py:84
  309.3 4.5 %copy-start.5 = (bf16[1,1,320,4096]{3,2,1,0:T(8,128)(2,1)S(1)}, bf16[1,1,320,4096]{3,2,1,0:T(8,128)(2,1)}, u32[]{:S(2)}) copy-start(bf16[1,1,320,4096]{3,2,1,0:T(8,128)(2,1)} %all-gather.3.cloned.1.call-done) | copy-start | bytes 7864324
  337.1 6.0 %copy-start.1 = (bf16[1,256,4096]{2,1,0:T(8,128)(2,1)S(1)}, bf16[1,256,4096]{2,1,0:T(8,128)(2,1)}, u32[]{:S(2)}) copy-start(bf16[1,256,4096]{2,1,0:T(8,128)(2,1)} %param.12) | copy-start | bytes 6291460
Sparse Core Ops, SparseCore 0:
  42.1 38.4 all-gather.4
  82.5 39.4 all-gather.2
Sparse Core Ops, SparseCore 1:
  66.7 48.8 reduce-scatter.1
where the time goes:
time: 352 us; the launch traced here: 350 us
  blocking collectives  87.6 us (25%)
  other arithmetic  80.1 us (23%)
  local copies, waits for them, and re-layouts  71.3 us (20%)
  waiting for transfers between devices  56.7 us (16%)
  matrix products  24.6 us (7%)
  between operations  15.7 us (4%)
  starting transfers between devices  14.4 us (4%)
    unnamed x1, other arithmetic  68.8 us
    all_gather x1, waiting for transfers between devices, local(): lax.all_gather(part_grads, 'tp', axis=3, tiled=True)  37.3 us
    psum x1, blocking collectives, local(): products = lax.psum(partial_products, 'tp')  33.7 us
    all_to_all x1, blocking collectives, local(): lax.all_to_all(sent_tokens, 'ep', split_axis=0, concat_axis=2, tiled=True)  24.5 us
    all_to_all x1, blocking collectives, local(): lax.all_to_all(sent_grads, 'ep', split_axis=0, concat_axis=2, tiled=True)  21.2 us
    unnamed x29, local copies, waits for them, and re-layouts  18.1 us
    all_to_all x1, waiting for transfers between devices, local(): lax.all_to_all(summed[None], 'ep', split_axis=2, concat_axis=0, tiled=True)  16.6 us
    convert_element_type x1, local copies, waits for them, and re-layouts, local(): partial_rows = partial_rows.astype(jnp.bfloat16)  14.3 us
  transfers between devices with their start and end apart: 6, of which 3 were waited for; matrix products, arithmetic and copies ran while one was open for 47% of the time, Pallas kernels for 0%

commit v1 on v0

--- a/solution.py
+++ b/solution.py
@@ -1,7 +1,17 @@
+import functools
 import jax
 import jax.numpy as jnp
 from jax import lax
 from jax.sharding import PartitionSpec as P
+
+
+def finish_the_turns(u_in, peer_axis):
+    mat_out = jnp.split(u_in, lax.axis_size(peer_axis), axis=2)
+    everything = lax.all_to_all(jnp.stack(mat_out), peer_axis, concat_axis=0, split_axis=0)
+    return jnp.concatenate(everything, axis=0)
+
+
+solve_quarters = functools.partial(finish_the_turns, peer_axis="tp")
 
 
 def slot_tables(routes, num_experts, capacity):
@@ -76,7 +86,7 @@
         "lrf,lfd->lrd", up_delta, up_proj, preferred_element_type=jnp.float32
     )
     partial_rows = partial_rows.astype(jnp.bfloat16)
-    gathered = lax.all_to_all(partial_rows, "tp", split_axis=2, concat_axis=0, tiled=True)
+    gathered = solve_quarters(partial_rows)
     gathered = gathered.reshape((tp_count,) + partial_rows.shape[:2] + (-1,))
     summed = jnp.sum(gathered, axis=0, dtype=jnp.float32)
     products = lax.psum(partial_products, "tp")

time: 352 us -> 233 us (0.66)
  other arithmetic: 80.1 us -> 9.95 us
  local copies, waits for them, and re-layouts: 71.3 us -> 22.9 us
  waiting for transfers between devices: 56.7 us -> 60.4 us
    unnamed x1 -> x0, other arithmetic: 68.8 us -> none
    convert_element_type x2 -> x0, local copies, waits for them, and re-layouts: 21.7 us -> none  [the longest x1 14.3 us: local(): partial_rows = partial_rows.astype(jnp.bfloat16)]
    all_to_all x1 -> x0, local copies, waits for them, and re-layouts: 14 us -> none  [local(): lax.all_to_all(partial_rows, 'tp', split_axis=2, concat_axis=0, tiled=True)]
    unnamed x29 -> x26, local copies, waits for them, and re-layouts: 18.1 us -> 5.17 us
  transfers between devices with their start and end apart: 6 -> 6, of which waited for: 3 -> 4; matrix products, arithmetic and copies ran while one was open for 47% -> 19% of each run, Pallas kernels for 0% -> 0%
where the time goes in v1:
time: 233 us; the launch traced here: 232 us
  blocking collectives  87.6 us (38%)
  waiting for transfers between devices  60.4 us (26%)
  local copies, waits for them, and re-layouts  22.9 us (10%)
  matrix products  22 us (9%)
  between operations  15.8 us (7%)
  starting transfers between devices  13.7 us (6%)
  other arithmetic  9.95 us (4%)
    all_gather x1, waiting for transfers between devices, local(): lax.all_gather(part_grads, 'tp', axis=3, tiled=True)  36.5 us
    psum x1, blocking collectives, local(): products = lax.psum(partial_products, 'tp')  33.7 us
    all_to_all x1, blocking collectives, local(): lax.all_to_all(sent_tokens, 'ep', split_axis=0, concat_axis=2, tiled=True)  24.5 us
    all_to_all x1, blocking collectives, local(): lax.all_to_all(sent_grads, 'ep', split_axis=0, concat_axis=2, tiled=True)  21.2 us
    all_to_all x1, waiting for transfers between devices, local(): lax.all_to_all(summed[None], 'ep', split_axis=2, concat_axis=0, tiled=True)  18.1 us
    all_to_all x1, blocking collectives, local(): lax.all_to_all(slot_weight, 'ep', split_axis=0, concat_axis=2, tiled=True)  8.11 us
    unnamed x26, local copies, waits for them, and re-layouts  5.17 us
  transfers between devices with their start and end apart: 6, of which 4 were waited for; matrix products, arithmetic and copies ran while one was open for 19% of the time, Pallas kernels for 0%

profile of v1, /device:TPU:0, one launch (start us, length us, event | category | flops | bytes accessed | tf_op | source)
XLA Modules:
  0.0 232.3 jit_solution(4868242754059209188)
XLA Ops:
  8.1 1.0 copy.36
  9.0 0.1 eq.26
  9.2 0.1 reshape.315
  9.3 0.6 reduce-window.6
  9.9 0.2 slice_reduce_fusion
  10.3 0.2 select_reduce_fusion
  10.4 0.2 fusion.23
  10.6 2.6 %gather_fusion.1 = bf16[320,1024]{1,0:T(8,128)(2,1)} fusion(bf16[128,1024]{1,0:T(8,128)(2,1)S(1)} %copy-done.1, s32[1024]{0:T(1024)S(1)} %get-tuple-element.42), kind=kCustom, calls=%fused_computation.1 | custom fusion | bytes 1312000 | tf_op jit(solution)/shard_map/gather | solution.py:47
  13.3 2.6 %gather_fusion.2 = bf16[320,1024]{1,0:T(8,128)(2,1)} fusion(bf16[128,1024]{1,0:T(8,128)(2,1)S(1)} %copy-done.2, s32[1024]{0:T(1024)S(1)} %get-tuple-element.42), kind=kCustom, calls=%fused_computation.2 | custom fusion | bytes 1312000 | tf_op jit(solution)/shard_map/gather | solution.py:46
  16.0 1.4 broadcast_select_fusion.1
  17.5 24.5 %all_to_all.56 = bf16[8,1,40,1024]{3,2,1,0:T(8,128)(2,1)} all-to-all(bf16[8,1,40,1024]{3,2,1,0:T(8,128)(2,1)S(1)} %get-tuple-element.41), channel_id=1, replica_groups=mesh['ep'=8,'tp'=4] {'ep'}, dimensions={0} | all-to-all | bytes 1310720 | tf_op jit(solution)/shard_map/all_to_all | solution.py:49
  42.1 21.2 %all_to_all.57 = bf16[8,1,40,1024]{3,2,1,0:T(8,128)(2,1)} all-to-all(bf16[8,1,40,1024]{3,2,1,0:T(8,128)(2,1)S(1)} %get-tuple-element.40), channel_id=1, replica_groups=mesh['ep'=8,'tp'=4] {'ep'}, dimensions={0} | all-to-all | bytes 1310720 | tf_op jit(solution)/shard_map/all_to_all | solution.py:50
  63.4 2.7 %fusion.30 = f32[1024,1024]{1,0:T(8,128)} fusion(bf16[128,1024]{1,0:T(8,128)(2,1)S(1)} %copy-done.8, bf16[128,1024]{1,0:T(8,128)(2,1)S(1)} %copy-done.1), kind=kOutput, calls=%fused_computation.73 | convolution fusion | flops 268435456 | bytes 4718592 | tf_op jit(solution)/shard_map/dot_general | solution.py:103
  66.1 0.7 copy-done.10
  66.9 0.1 reshape.317
  67.0 2.4 %gather_fusion = bf16[320]{0:T(512)(128)(2,1)S(1)} fusion(bf16[256]{0:T(256)(128)(2,1)S(1)} %reshape.317, s32[1024]{0:T(1024)S(1)} %get-tuple-element.43), kind=kCustom, calls=%fused_computation | custom fusion | bytes 2560 | tf_op jit(solution)/shard_map/gather | solution.py:43
  69.5 8.1 %all_to_all.58 = bf16[8,1,40]{2,1,0:T(2,128)(2,1)S(1)} all-to-all(bf16[8,1,40]{2,1,0:T(2,128)(2,1)S(1)} %convert_element_type.102), channel_id=1, replica_groups=mesh['ep'=8,'tp'=4] {'ep'}, dimensions={0} | all-to-all | bytes 1280 | tf_op jit(solution)/shard_map/all_to_all | solution.py:51
  77.7 2.9 %all-gather.5.cloned.1.call-done = bf16[1,1,320,4096]{3,2,1,0:T(8,128)(2,1)} async-done(((bf16[1,1,320,1024]{3,2,1,0:T(8,128)(2,1)}), bf16[1,1,320,4096]{3,2,1,0:T(8,128)(2,1)}) %all-gather.5.cloned.1.call-update) | async-done | bytes 2621456 | tf_op jit(solution)/shard_map/all_gather | solution.py:54
  80.6 2.8 %fusion.7 = f32[320,256]{1,0:T(8,128)S(1)} fusion(bf16[1,1,320,4096]{3,2,1,0:T(8,128)(2,1)} %all-gather.5.cloned.1.call-done, bf16[1,256,4096]{2,1,0:T(8,128)(2,1)S(1)} %copy-done), kind=kOutput, calls=%fused_computation.18 | convolution fusion | flops 671088640 | bytes 5046272 | tf_op jit(solution)/shard_map/lrd,lfd->lrf/dot_general | solution.py:60
  83.4 0.4 copy-done.6
  83.9 1.6 fusion.9
  85.5 36.5 %all-gather.3.cloned.1.call-done = bf16[1,1,320,4096]{3,2,1,0:T(8,128)(2,1)} async-done(((bf16[1,1,320,1024]{3,2,1,0:T(8,128)(2,1)}), bf16[1,1,320,4096]{3,2,1,0:T(8,128)(2,1)}) %all-gather.3.cloned.1.call-update) | async-done | bytes 2621456 | tf_op jit(solution)/shard_map/all_gather | solution.py:55
  122.0 3.4 %fusion.20 = (f32[320]{0:T(512)S(1)}, bf16[320,256]{1,0:T(8,128)(2,1)S(1)}, bf16[320,256]{1,0:T(8,128)(2,1)S(1)}, bf16[320,256]{1,0:T(8,128)(2,1)S(1)}) fusion(f32[320,256]{1,0:T(8,128)} %fusion.9, f32[320,256]{1,0:T(8,128)S(1)} %fusion.7, f32[320]{0:T(512)S(1)} %reshape.328, bf16[1,256,4096]{2,1,0:T(8,128)(2,1)} %param.14, ...), kind=kOutput, calls=%fused_computation.40 | convolution fusion | flops 672644800 | bytes 5868032 | tf_op jit(solution)/shard_map/lrd,lfd->lrf/dot_general | solution.py:65
  125.4 0.8 fusion.14
  126.3 0.7 copy-done.7
  127.0 0.9 fusion.1
  127.9 0.3 slice_bitcast_fusion.3
  128.2 1.9 pad_maximum_fusion
  130.0 4.5 %all-to-all-start.3 = ((bf16[4,1,320,1024]{3,2,1,0:T(8,128)(2,1)}), bf16[4,1,320,1024]{3,2,1,0:T(8,128)(2,1)}, u32[]{:S(2)}, u32[]{:S(2)}) async-start(bf16[4,1,320,1024]{3,2,1,0:T(8,128)(2,1)} %pad_maximum_fusion), calls=%async_computation.3 | async-start | bytes 5242880 | tf_op jit(solution)/shard_map/all_to_all | solution.py:10
  134.6 33.7 %psum.7 = f32[1,1,320]{2,1,0:T(1,128)S(1)} all-reduce(f32[1,1,320]{2,1,0:T(1,128)S(1)} %broadcast_in_dim.48), channel_id=1, replica_groups=mesh['ep'=8,'tp'=4] {'tp'}, use_global_device_ids=true, to_apply=%region_8.9 | all-reduce | flops 320 | bytes 2560 | tf_op jit(solution)/shard_map/psum | solution.py:92
  168.3 0.8 copy.43
  169.1 4.6 %all-to-all-start.5 = ((f32[1,1,320]{1,0,2:T(1,128)}), f32[1,1,320]{1,0,2:T(1,128)S(1)}, u32[]{:S(2)}, u32[]{:S(2)}) async-start(f32[1,1,320]{1,0,2:T(1,128)} %copy.43), calls=%async_computation.5 | async-start | bytes 327680 | tf_op jit(solution)/shard_map/all_to_all | solution.py:95
  173.7 2.4 %convert_reduce_fusion = f32[320,1024]{1,0:T(8,128)S(1)} fusion(bf16[4,1,320,1024]{3,2,1,0:T(8,128)(2,1)} %all-to-all-done.3), kind=kLoop, calls=%fused_computation.7 | loop fusion | flops 2293760 | bytes 3932160 | tf_op jit(solution)/shard_map/reduce_sum | solution.py:91
  176.1 2.0 broadcast_in_dim.47
  178.1 2.8 %all-to-all-done.5 = f32[1,1,320]{1,0,2:T(1,128)S(1)} async-done(((f32[1,1,320]{1,0,2:T(1,128)}), f32[1,1,320]{1,0,2:T(1,128)S(1)}, u32[]{:S(2)}, u32[]{:S(2)}) %all-to-all-start.5) | async-done | bytes 1312 | tf_op jit(solution)/shard_map/all_to_all | solution.py:95
  180.9 4.5 %all-to-all-start.4 = ((f32[1,1,320,1024]{3,1,0,2:T(1,128)}), f32[1,1,320,1024]{3,1,0,2:T(1,128)}, u32[]{:S(2)}, u32[]{:S(2)}) async-start(f32[1,1,320,1024]{3,1,0,2:T(1,128)} %broadcast_in_dim.47), calls=%async_computation.4 | async-start | bytes 2621440 | tf_op jit(solution)/shard_map/all_to_all | solution.py:94
  185.5 0.1 mul.88
  185.7 4.5 %fusion.2 = bf16[1,256,4096]{2,1,0:T(8,128)(2,1)} fusion(bf16[320,256]{1,0:T(8,128)(2,1)S(1)} %get-tuple-element.38, bf16[1,1,320,4096]{3,2,1,0:T(8,128)(2,1)} %all-gather.5.cloned.1.call-done), kind=kOutput, calls=%fused_computation.12 | convolution fusion | flops 672137216 | bytes 4882432 | tf_op jit(solution)/shard_map/lrf,lrd->lfd/dot_general | solution.py:73
  190.2 2.6 %fusion.3 = bf16[1,256,4096]{2,1,0:T(8,128)(2,1)} fusion(bf16[320,256]{1,0:T(8,128)(2,1)S(1)} %get-tuple-element.39, bf16[1,1,320,4096]{3,2,1,0:T(8,128)(2,1)S(1)} %copy-done.4), kind=kOutput, calls=%fused_computation.13 | convolution fusion | flops 672137216 | bytes 4882432 | tf_op jit(solution)/shard_map/lrf,lrd->lfd/dot_general | solution.py:76
  192.8 2.7 %fusion.4 = bf16[1,256,4096]{2,1,0:T(8,128)(2,1)} fusion(bf16[1,1,320,4096]{3,2,1,0:T(8,128)(2,1)S(1)} %copy-done.5, bf16[320,256]{1,0:T(8,128)(2,1)S(1)} %get-tuple-element.33, f32[320]{0:T(512)S(1)} %reshape.328), kind=kOutput, calls=%fused_computation.14 | convolution fusion | flops 672382976 | bytes 4883712 | tf_op jit(solution)/shard_map/lrf,lrd->lfd/dot_general | solution.py:79
  195.5 1.1 reduce.7
  196.5 1.9 gather_fusion.4
  198.6 0.6 copy.44
  199.3 18.1 %all-to-all-done.4 = f32[1,1,320,1024]{3,1,0,2:T(1,128)} async-done(((f32[1,1,320,1024]{3,1,0,2:T(1,128)}), f32[1,1,320,1024]{3,1,0,2:T(1,128)}, u32[]{:S(2)}, u32[]{:S(2)}) %all-to-all-start.4) | async-done | bytes 1310752 | tf_op jit(solution)/shard_map/all_to_all | solution.py:94
  217.4 1.6 copy.47
  219.0 2.0 gather_fusion.3
  221.0 1.8 reshape.324
  222.8 2.1 reduce_sum.56
  (46 shorter events, 1.1 us)
Async XLA Ops:
  8.0 72.6 %copy-start = (bf16[1,256,4096]{2,1,0:T(8,128)(2,1)S(1)}, bf16[1,256,4096]{2,1,0:T(8,128)(2,1)}, u32[]{:S(2)}) copy-start(bf16[1,256,4096]{2,1,0:T(8,128)(2,1)} %param.12) | copy-start | bytes 6291460
  8.0 2.6 %copy-start.1 = (bf16[128,1024]{1,0:T(8,128)(2,1)S(1)}, bf16[128,1024]{1,0:T(8,128)(2,1)}, u32[]{:S(2)}) copy-start(bf16[128,1024]{1,0:T(8,128)(2,1)} %param.9) | copy-start | bytes 786436
  8.0 72.6 %all-gather.5.cloned.1.call-start = ((), (), s32[]{:S(2)}) async-start(), calls=%async_computation.8 | async-start | bytes 3276800 | tf_op jit(solution)/shard_map/all_gather | solution.py:54
  10.6 2.7 %copy-start.2 = (bf16[128,1024]{1,0:T(8,128)(2,1)S(1)}, bf16[128,1024]{1,0:T(8,128)(2,1)}, u32[]{:S(2)}) copy-start(bf16[128,1024]{1,0:T(8,128)(2,1)} %param.8) | copy-start | bytes 786436
  17.5 45.9 %copy-start.8 = (bf16[128,1024]{1,0:T(8,128)(2,1)S(1)}, bf16[128,1024]{1,0:T(8,128)(2,1)}, u32[]{:S(2)}) copy-start(bf16[128,1024]{1,0:T(8,128)(2,1)} %param.15) | copy-start | bytes 786436
  42.0 80.0 %all-gather.3.cloned.1.call-start = ((), (), s32[]{:S(2)}) async-start(), calls=%async_computation.7 | async-start | bytes 3276800 | tf_op jit(solution)/shard_map/all_gather | solution.py:55
  63.3 161.6 %reduce-scatter.2.cloned.1.call-start = ((), (), s32[]{:S(2)}) async-start(), calls=%async_computation.9 | async-start | bytes 4718592 | tf_op jit(solution)/shard_map/reduce_scatter | solution.py:102
  66.0 0.7 copy-start.10
  80.6 2.8 %copy-start.3 = (bf16[1,1,320,4096]{3,2,1,0:T(8,128)(2,1)S(1)}, bf16[1,1,320,4096]{3,2,1,0:T(8,128)(2,1)}, u32[]{:S(2)}) copy-start(bf16[1,1,320,4096]{3,2,1,0:T(8,128)(2,1)} %all-gather.5.cloned.1.call-done) | copy-start | bytes 7864324
  80.6 3.2 %copy-start.6 = (bf16[1,256,4096]{2,1,0:T(8,128)(2,1)S(1)}, bf16[1,256,4096]{2,1,0:T(8,128)(2,1)}, u32[]{:S(2)}) copy-start(bf16[1,256,4096]{2,1,0:T(8,128)(2,1)} %param.13) | copy-start | bytes 6291460
  125.4 1.6 copy-start.7
  130.0 39.1 %all-to-all-start.3 = ((bf16[4,1,320,1024]{3,2,1,0:T(8,128)(2,1)}), bf16[4,1,320,1024]{3,2,1,0:T(8,128)(2,1)}, u32[]{:S(2)}, u32[]{:S(2)}) async-start(bf16[4,1,320,1024]{3,2,1,0:T(8,128)(2,1)} %pad_maximum_fusion), calls=%async_computation.3 | async-start | bytes 5242880 | tf_op jit(solution)/shard_map/all_to_all | solution.py:10
  169.1 11.8 %all-to-all-start.5 = ((f32[1,1,320]{1,0,2:T(1,128)}), f32[1,1,320]{1,0,2:T(1,128)S(1)}, u32[]{:S(2)}, u32[]{:S(2)}) async-start(f32[1,1,320]{1,0,2:T(1,128)} %copy.43), calls=%async_computation.5 | async-start | bytes 327680 | tf_op jit(solution)/shard_map/all_to_all | solution.py:95
  176.1 9.2 %copy-start.9 = (s32[128,2]{0,1:T(2,128)S(1)}, s32[128,2]{0,1:T(2,128)}, u32[]{:S(2)}) copy-start(s32[128,2]{0,1:T(2,128)} %param.10) | copy-start | bytes 3076
  180.9 36.5 %all-to-all-start.4 = ((f32[1,1,320,1024]{3,1,0,2:T(1,128)}), f32[1,1,320,1024]{3,1,0,2:T(1,128)}, u32[]{:S(2)}, u32[]{:S(2)}) async-start(f32[1,1,320,1024]{3,1,0,2:T(1,128)} %broadcast_in_dim.47), calls=%async_computation.4 | async-start | bytes 2621440 | tf_op jit(solution)/shard_map/all_to_all | solution.py:94
  185.7 4.5 %copy-start.4 = (bf16[1,1,320,4096]{3,2,1,0:T(8,128)(2,1)S(1)}, bf16[1,1,320,4096]{3,2,1,0:T(8,128)(2,1)}, u32[]{:S(2)}) copy-start(bf16[1,1,320,4096]{3,2,1,0:T(8,128)(2,1)} %all-gather.5.cloned.1.call-done) | copy-start | bytes 7864324
  190.2 2.6 %copy-start.5 = (bf16[1,1,320,4096]{3,2,1,0:T(8,128)(2,1)S(1)}, bf16[1,1,320,4096]{3,2,1,0:T(8,128)(2,1)}, u32[]{:S(2)}) copy-start(bf16[1,1,320,4096]{3,2,1,0:T(8,128)(2,1)} %all-gather.3.cloned.1.call-done) | copy-start | bytes 7864324
Sparse Core Ops, SparseCore 0:
  42.1 38.4 all-gather.4
  82.5 39.4 all-gather.2
Sparse Core Ops, SparseCore 1:
  66.7 48.8 reduce-scatter.1
